TPU v7x, 32 devices: a whole 2x2x4 slice. The times are simulated.
32 devices in a mesh: dp: 2 (over x), kv: 8 (over z, y), tp: 2 (over core).
Axes of the slice: x: 2, y: 2, z: 4, core: 2. Of those that a mesh axis runs over, the one named last changes fastest.
Arguments:
- tokens: bfloat16 [128, 4096], P('dp', 'kv'), may hold values from -6 to 6
- norm_gain: float32 [4096], P('kv'), may hold values from 0.1 to 1.9
- w_query: bfloat16 [4096, 2048], P('kv', 'tp'), may hold values from -0.09375 to 0.09375
- w_key: bfloat16 [4096, 2048], P('kv', 'tp'), may hold values from -0.09375 to 0.09375
- w_value: bfloat16 [4096, 2048], P('kv', 'tp'), may hold values from -0.09375 to 0.09375
- query_gain: float32 [64], replicated, may hold values from 0.1 to 1.9
- key_gain: float32 [64], replicated, may hold values from 0.1 to 1.9
- head_bias: float32 [32], P('tp'), may hold values from -11 to -3
- w_output: bfloat16 [2048, 4096], P('tp', 'kv'), may hold values from -0.125 to 0.125
- cache_keys: bfloat16 [8, 2048, 2048], P('dp', 'kv', 'tp'), may hold values from -6 to 6
- cache_values: bfloat16 [8, 2048, 2048], P('dp', 'kv', 'tp'), may hold values from -6 to 6
- base_length: int32 [8], P('dp'), may hold values from 1536 to 2016
- accepted: int32 [8], P('dp'), may hold values from 0 to 16
- parents: int32 [8, 16], P('dp'), may hold values from -1 to 14, as said below
Outputs:
- layer_out: bfloat16 [128, 4096], P('dp', 'kv')
- updated_keys: bfloat16 [8, 2048, 2048], P('dp', 'kv', 'tp')
- updated_values: bfloat16 [8, 2048, 2048], P('dp', 'kv', 'tp')
Inputs may be any that keep to these rules, and one draw needn't show every extreme that they name: base_length + accepted + 16 <= 2048 for every sequence. parents[s, i] is -1 or a proposal before i; parents[s, 0] is -1.
All inputs are finite; a program needn't handle non-finite values.
Results may differ from a plain program's by a relative error of at most 0.00175.
The roundings to bfloat16 on the way count: a program that leaves them out, or rounds other values in their place, can miss the bound.
Values may be sent and summed in bfloat16 or wider, within the bound.
A program may use at most 64 MiB of HBM per device.

v0:
```python
import jax
import jax.numpy as jnp
from jax import lax
from jax.sharding import PartitionSpec as P

D = 4096
HEAD_DIM = 64


epsilon = 1e-05


def carried_in(value, axis, join, neutral):
    count, mine = (lax.axis_size(axis), lax.axis_index(axis))
    pieces = lax.all_gather(value, axis)
    pieces = pieces[::-1]
    mine = count - 1 - mine
    running = jnp.full_like(value, 0) + jnp.asarray(neutral, value.dtype)

    def step(position, running):
        longer = join(running, pieces[position])
        return jnp.where(position < mine, longer, running)

    return lax.fori_loop(0, count - 1, step, running)


def head_norm(raw, gain):
    grouped = raw.reshape(raw.shape[0], -1, gain.shape[0])
    factor = lax.rsqrt(jnp.mean(grouped * grouped, axis=2, keepdims=True) + epsilon)
    return (grouped * factor * gain).reshape(raw.shape).astype(jnp.bfloat16)


def ancestry(parents):
    width = parents.shape[-1]
    direct = (parents[..., :, None] == jnp.arange(width, dtype=jnp.int32)).astype(jnp.float32)

    def extend(step, above):
        return direct + jnp.einsum("sij,sjk->sik", direct, above)

    return lax.fori_loop(0, width - 1, extend, direct)


def later_sum(values):
    length = values.shape[-1]
    order = jnp.arange(length, dtype=jnp.int32)
    after = (order[:, None] > order[None, :]).astype(jnp.float32)
    return jnp.einsum("shqp,pr->shqr", values, after, precision=lax.Precision.HIGHEST)


def finish(query_raw, key_raw, value_raw, squares, query_gain, key_gain):
    inv_rms = lax.rsqrt(squares / D + epsilon)
    queries = head_norm(query_raw, query_gain)
    new_keys = head_norm(key_raw, key_gain)
    new_values = (value_raw * inv_rms[:, None]).astype(jnp.bfloat16)
    return (queries, new_keys, new_values)


def shards(
    tokens,
    norm_gain,
    w_query,
    w_key,
    w_value,
    query_gain,
    key_gain,
    head_bias,
    w_output,
    cache_keys,
    cache_values,
    base_length,
    accepted,
    parents,
):
    wide = tokens.astype(jnp.float32)
    scaled = (wide * norm_gain).astype(jnp.bfloat16)
    squares = jnp.sum(wide * wide, axis=1)
    query_part = jnp.dot(scaled, w_query, preferred_element_type=jnp.float32)
    key_part = jnp.dot(scaled, w_key, preferred_element_type=jnp.float32)
    value_part = jnp.dot(scaled, w_value, preferred_element_type=jnp.float32)
    query_raw, key_raw, value_raw, row_squares = lax.psum(
        (query_part, key_part, value_part, squares), "kv"
    )
    queries, new_keys, new_values = finish(
        query_raw, key_raw, value_raw, row_squares, query_gain, key_gain
    )
    seq_dev, width = parents.shape
    local_heads = head_bias.shape[0]
    span = cache_keys.shape[1]
    factor = HEAD_DIM ** (-0.5)
    shape_four = (seq_dev, width, local_heads, HEAD_DIM)
    query_heads = queries.reshape(shape_four)
    key_heads = new_keys.reshape(shape_four)
    value_heads = new_values.reshape(shape_four)
    stored_k = cache_keys.reshape(seq_dev, span, local_heads, HEAD_DIM)
    stored_v = cache_values.reshape(seq_dev, span, local_heads, HEAD_DIM)
    valid = base_length + accepted
    positions = lax.axis_index("kv") * span + jnp.arange(span, dtype=jnp.int32)
    live = (positions[None, :] < valid[:, None])[:, None, None, :]
    score = jnp.einsum("sqhd,sphd->shqp", query_heads, stored_k, preferred_element_type=jnp.float32)
    score = score * factor + head_bias[None, :, None, None]
    stay = jnp.where(live, jax.nn.log_sigmoid(-score), 0.0)
    tail = later_sum(stay)
    weight = jnp.where(live, jnp.exp(jax.nn.log_sigmoid(score) + tail), 0.0).astype(jnp.bfloat16)
    block_sum = jnp.einsum("shqp,sphd->sqhd", weight, stored_v, preferred_element_type=jnp.float32)
    block_log = jnp.sum(stay, axis=3)
    later = carried_in(block_log, "kv", jnp.add, jnp.zeros_like(block_log))
    weighted = block_sum * jnp.exp(jnp.swapaxes(later, 1, 2))[..., None]
    cache_part = lax.psum(weighted, "kv")
    mine = (ancestry(parents) > 0.5)[:, None, :, :]
    inner = jnp.einsum(
        "sqhd,sjhd->shqj", query_heads, key_heads, preferred_element_type=jnp.float32
    )
    inner = inner * factor + head_bias[None, :, None, None]
    stay_tree = jnp.where(mine, jax.nn.log_sigmoid(-inner), 0.0)
    tail_tree = later_sum(stay_tree)
    weight_tree = jnp.where(mine, jnp.exp(jax.nn.log_sigmoid(inner) + tail_tree), 0.0).astype(
        jnp.bfloat16
    )
    ancestor_sum = jnp.einsum(
        "shqj,sjhd->sqhd", weight_tree, value_heads, preferred_element_type=jnp.float32
    )
    ancestor_log = jnp.sum(stay_tree, axis=3)
    attended = ancestor_sum + jnp.exp(jnp.swapaxes(ancestor_log, 1, 2))[..., None] * cache_part
    attended = attended.astype(jnp.bfloat16).reshape(seq_dev * width, local_heads * HEAD_DIM)
    mix_part = jnp.dot(attended, w_output, preferred_element_type=jnp.float32)
    mix = lax.psum(mix_part, "tp")
    out_squares = lax.psum(jnp.sum(mix * mix, axis=1), "kv")
    layer_out = (mix * lax.rsqrt(out_squares / D + epsilon)[:, None]).astype(jnp.bfloat16)
    offset = positions[None, :] - valid[:, None]
    inside = ((offset >= 0) & (offset < width))[:, :, None]
    chooser = (offset[:, :, None] == jnp.arange(width, dtype=jnp.int32)).astype(jnp.bfloat16)
    fresh = jnp.concatenate(
        (new_keys.reshape(seq_dev, width, -1), new_values.reshape(seq_dev, width, -1)), axis=2
    )
    placed = jnp.einsum("spi,sic->spc", chooser, fresh, preferred_element_type=jnp.float32).astype(
        jnp.bfloat16
    )
    half = cache_keys.shape[2]
    updated_keys = jnp.where(inside, placed[:, :, :half], cache_keys)
    updated_values = jnp.where(inside, placed[:, :, half:], cache_values)
    return (layer_out, updated_keys, updated_values)


def solution(mesh):
    return jax.shard_map(
        shards,
        mesh=mesh,
        in_specs=(
            P("dp", "kv"),
            P("kv"),
            P("kv", "tp"),
            P("kv", "tp"),
            P("kv", "tp"),
            P(),
            P(),
            P("tp"),
            P("tp", "kv"),
            P("dp", "kv", "tp"),
            P("dp", "kv", "tp"),
            P("dp"),
            P("dp"),
            P("dp", None),
        ),
        out_specs=(P("dp", "kv"), P("dp", "kv", "tp"), P("dp", "kv", "tp")),
        check_vma=False,
    )
```

profile of v0, /device:TPU:0, one launch (start us, length us, event | category | flops | bytes accessed | tf_op | source)
XLA Modules:
  0.0 288.7 jit_solution(6623477936050046395)
XLA Ops:
  7.3 1.1 copy-done
  8.4 1.9 fusion.42
  11.1 13.2 %while.25 = (s32[]{:T(128)}, f32[4,16,16]{2,1,0:T(8,128)S(1)}, s32[4,16]{1,0:T(4,128)}, s32[]{:T(128)}) while((s32[]{:T(128)}, f32[4,16,16]{2,1,0:T(8,128)S(1)}, s32[4,16]{1,0:T(4,128)}, s32[]{:T(128)}) %tuple.59), condition=%wide.region_4.0_spmd.clone, body=%wide.region_3.0_spmd.clone.sunk | while | flops 35842 | bytes 16693 | solution.py:40
  11.1 0.9 convolution_add_fusion.4
  12.0 0.9 convolution_add_fusion.4
  12.9 0.9 convolution_add_fusion.4
  13.8 0.9 convolution_add_fusion.4
  14.6 0.9 convolution_add_fusion.4
  15.5 0.9 convolution_add_fusion.4
  16.4 0.9 convolution_add_fusion.4
  17.3 0.9 convolution_add_fusion.4
  18.2 0.9 convolution_add_fusion.4
  19.0 0.9 convolution_add_fusion.4
  19.9 0.9 convolution_add_fusion.4
  20.8 0.9 convolution_add_fusion.4
  21.7 0.9 convolution_add_fusion.4
  22.6 0.9 convolution_add_fusion.4
  23.5 0.9 convolution_add_fusion.4
  24.3 2.3 fusion.40
  27.4 2.5 copy.41
  29.9 3.9 %copy.43 = bf16[4,256,1024]{1,2,0:T(8,128)(2,1)} copy(bf16[4,256,1024]{2,1,0:T(8,128)(2,1)} %param.28) | data formatting | bytes 4194304 | tf_op args[10]
  33.9 2.2 fusion.44
  36.1 49.1 %all-reduce.5.cloned.1.call-done = f32[64,1024]{1,0:T(8,128)} async-done(((f32[64,1024]{1,0:T(8,128)}), f32[64,1024]{1,0:T(8,128)}) %all-reduce.5.cloned.1.call-update) | async-done | bytes 262160 | tf_op jit(solution)/shard_map/psum | solution.py:80
  85.2 1.8 mul.126
  87.1 1.9 mul.127
  89.0 1.9 reduce_sum.55
  90.8 0.8 add_rsqrt_fusion.1
  91.6 1.0 mul.128
  92.6 1.9 mul.129
  94.5 1.6 multiply_convert_fusion.1
  96.1 1.1 reshape.148
  97.3 2.1 fusion.17
  100.1 2.7 fusion.7
  102.8 30.9 %all-gather = f32[32,16,16]{2,1,0:T(8,128)S(1)} all-gather(f32[4,16,16]{2,1,0:T(8,128)S(1)} %fusion.16), channel_id=2, replica_groups=mesh['dp'=2,'kv'=8,'tp'=2] {'kv'}, dimensions={0}, use_global_device_ids=true | all-gather | bytes 36864 | tf_op jit(solution)/shard_map/all_gather | solution.py:15
  134.4 5.4 %while.26 = (s32[]{:T(128)}, f32[4,16,16]{2,1,0:T(8,128)S(1)}, s32[]{:T(128)}, f32[8,4,16,16]{3,2,1,0:T(8,128)}, s32[]{:T(128)}, /*index=5*/s32[]{:T(128)}) while((s32[]{:T(128)}, f32[4,16,16]{2,1,0:T(8,128)S(1)}, s32[]{:T(128)}, f32[8,4,16,16]{3,2,1,0:T(8,128)}, s32[]{:T(128)}, /*index=5*/s32[]{:T(128)}) %tuple.56), condition=%wide.region_12.13_spmd.clone, body=%wide.region_11.12_spmd.clone.sunk | while | flops 3076 | bytes 12389 | solution.py:24
  134.4 0.8 add_select_fusion.2
  135.2 0.8 add_select_fusion.2
  135.9 0.8 add_select_fusion.2
  136.7 0.8 add_select_fusion.2
  137.5 0.8 add_select_fusion.2
  138.2 0.8 add_select_fusion.2
  139.0 0.8 add_select_fusion.2
  139.8 3.2 %fusion.11 = f32[4,16,16,64]{3,1,2,0:T(8,128)} fusion(bf16[4,16,16,256]{3,2,1,0:T(8,128)(2,1)} %fusion.7, bf16[4,256,16,64]{1,3,2,0:T(8,128)(2,1)} %bitcast.47, f32[4,16,16]{1,2,0:T(8,128)S(1)} %exponential_bitcast_fusion), kind=kOutput, calls=%fused_computation.23 | convolution fusion | flops 33619968 | bytes 2887680 | tf_op jit(solution)/shard_map/shqp,sphd->sqhd/dot_general | solution.py:104
  143.3 20.1 %psum.50 = f32[64]{0:T(128)S(1)} all-reduce(f32[64]{0:T(128)S(1)} %fusion.38), channel_id=1, replica_groups=mesh['dp'=2,'kv'=8,'tp'=2] {'kv'}, use_global_device_ids=true, to_apply=%region_2.0 | all-reduce | flops 64 | bytes 512 | tf_op jit(solution)/shard_map/psum | solution.py:80
  164.0 56.9 %all-reduce.9.cloned.1.call-done = (f32[64,1024]{1,0:T(8,128)}, f32[4,16,16,64]{3,1,2,0:T(8,128)}, f32[64,1024]{1,0:T(8,128)}) async-done(((f32[64,1024]{1,0:T(8,128)}, f32[4,16,16,64]{3,1,2,0:T(8,128)}, f32[64,1024]{1,0:T(8,128)}), (f32[64,1024]{1,0:T(8,128)}, f32[4,16,16,64]{3,1,2,0:T(8,128)}, f32[64,1024]{1,0:T(8,128)})) %all-reduce.9.cloned.1.call-update) | async-done | bytes 786448 | tf_op jit(solution)/shard_map/psum | solution.py:80
  220.9 1.8 mul.135
  222.8 1.9 mul.136
  224.6 1.3 reduce_sum.56
  225.9 1.0 mul.137
  226.9 1.9 mul.138
  228.8 1.0 multiply_convert_fusion
  230.0 1.2 fusion.23
  231.7 1.7 fusion.13
  233.5 0.9 reshape.147
  234.4 1.5 fusion.14
  235.9 0.8 copy.44
  236.7 1.1 reshape.152
  237.9 2.2 fusion.55
  240.1 1.3 convolution_convert_fusion
  241.7 2.3 slice_select_fusion
  243.9 13.9 %all-reduce.7.cloned.1.call-done = f32[64,512]{1,0:T(8,128)} async-done(((f32[64,512]{1,0:T(8,128)}), f32[64,512]{1,0:T(8,128)}) %all-reduce.7.cloned.1.call-update) | async-done | bytes 131088 | tf_op jit(solution)/shard_map/psum | solution.py:126
  257.8 1.0 multiply_reduce_fusion
  258.9 21.7 %psum.55 = f32[64]{0:T(128)S(1)} all-reduce(f32[64]{0:T(128)S(1)} %multiply_reduce_fusion), channel_id=1, replica_groups=mesh['dp'=2,'kv'=8,'tp'=2] {'kv'}, use_global_device_ids=true, to_apply=%region_16.17 | all-reduce | flops 64 | bytes 512 | tf_op jit(solution)/shard_map/psum | solution.py:127
  280.5 1.6 multiply_convert_fusion.3
  (83 shorter events, 5.1 us)
Async XLA Ops:
  7.2 1.2 copy-start
  7.2 17.2 %copy-start.6 = (bf16[64,512]{1,0:T(8,128)(2,1)S(1)}, bf16[64,512]{1,0:T(8,128)(2,1)}, u32[]{:S(2)}) copy-start(bf16[64,512]{1,0:T(8,128)(2,1)} %param.18) | copy-start | bytes 196612
  7.2 17.1 %copy-start.8 = (f32[512]{0:T(512)S(1)}, f32[512]{0:T(512)}, u32[]{:S(2)}) copy-start(f32[512]{0:T(512)} %param.19) | copy-start | bytes 6148
  7.2 19.4 %copy-start.19 = (s32[4]{0:T(128)S(1)}, s32[4]{0:T(128)}, u32[]{:S(2)}) copy-start(s32[4]{0:T(128)} %param.30) | copy-start | bytes 52
  7.2 19.4 %copy-start.18 = (s32[4]{0:T(128)S(1)}, s32[4]{0:T(128)}, u32[]{:S(2)}) copy-start(s32[4]{0:T(128)} %param.29) | copy-start | bytes 52
  7.2 20.0 %copy-start.16 = (f32[64]{0:T(128)S(1)}, f32[64]{0:T(128)}, u32[]{:S(2)}) copy-start(f32[64]{0:T(128)} %param.23) | copy-start | bytes 772
  7.2 20.1 %copy-start.17 = (f32[64]{0:T(128)S(1)}, f32[64]{0:T(128)}, u32[]{:S(2)}) copy-start(f32[64]{0:T(128)} %param.24) | copy-start | bytes 772
  7.2 20.1 %copy-start.1 = (bf16[4,256,1024]{2,1,0:T(8,128)(2,1)S(1)}, bf16[4,256,1024]{2,1,0:T(8,128)(2,1)}, u32[]{:S(2)}) copy-start(bf16[4,256,1024]{2,1,0:T(8,128)(2,1)} %param.27) | copy-start | bytes 6291460
  7.3 78.0 %all-reduce.5.cloned.1.call-start = ((), (), s32[]{:S(2)}) async-start(), calls=%async_computation | async-start | bytes 524288 | tf_op jit(solution)/shard_map/psum | solution.py:80
  10.3 210.6 %all-reduce.9.cloned.1.call-start = ((), (), s32[]{:S(2)}) async-start(), calls=%async_computation.2 | async-start | bytes 2097152 | tf_op jit(solution)/shard_map/psum | solution.py:80
  10.3 16.9 %copy-start.10 = (s32[256]{0:T(256)}, s32[256]{0:T(256)S(1)}, u32[]{:S(2)}) copy-start(s32[256]{0:T(256)S(1)} %iota_add_fusion) | copy-start | bytes 3076
  26.6 0.6 copy-start.12
  85.2 9.3 %copy-start.3 = (f32[64,1024]{1,0:T(8,128)S(1)}, f32[64,1024]{1,0:T(8,128)}, u32[]{:S(2)}) copy-start(f32[64,1024]{1,0:T(8,128)} %all-reduce.5.cloned.1.call-done) | copy-start | bytes 786436
  87.1 10.2 %copy-start.14 = (f32[16]{0:T(128)S(1)}, f32[16]{0:T(128)}, u32[]{:S(2)}) copy-start(f32[16]{0:T(128)} %param.25) | copy-start | bytes 196
  97.2 2.9 copy-start.5
  139.8 24.2 %copy-start.11 = (s32[256]{0:T(256)S(1)}, s32[256]{0:T(256)}, u32[]{:S(2)}) copy-start(s32[256]{0:T(256)} %copy-done.10) | copy-start | bytes 3076
  139.8 24.2 %copy-start.13 = (s32[4]{0:T(128)S(1)}, s32[4]{0:T(128)}, u32[]{:S(2)}) copy-start(s32[4]{0:T(128)} %copy-done.12) | copy-start | bytes 52
  143.1 114.8 %all-reduce.7.cloned.1.call-start = ((), (), s32[]{:S(2)}) async-start(), calls=%async_computation.1 | async-start | bytes 262144 | tf_op jit(solution)/shard_map/psum | solution.py:126
  220.9 7.9 %copy-start.4 = (f32[64,1024]{1,0:T(8,128)S(1)}, f32[64,1024]{1,0:T(8,128)}, u32[]{:S(2)}) copy-start(f32[64,1024]{1,0:T(8,128)} %get-tuple-element.139) | copy-start | bytes 786436
  231.2 2.2 copy-start.7
  231.2 2.2 copy-start.15
  240.1 1.6 copy-start.2
  240.1 1.6 copy-start.9
Sparse Core Ops, SparseCore 0:
  11.4 73.7 all-reduce.4
  143.2 77.6 all-reduce.8
  240.2 17.5 all-reduce.6
where the time goes:
time: 291 us; the launch traced here: 289 us
  waiting for transfers between devices  120 us (41%)
  blocking collectives  72.6 us (25%)
  matrix products  35.5 us (12%)
  other arithmetic  23.7 us (8%)
  local copies, waits for them, and re-layouts  22.6 us (8%)
  between operations  14 us (5%)
    psum x2, waiting for transfers between devices, shards(): lax.psum((query_part, key_part, value_part, squares), 'kv')  106 us
    all_gather x1, blocking collectives, carried_in(): pieces = lax.all_gather(value, axis)  30.9 us
    psum x1, blocking collectives, shards(): out_squares = lax.psum(jnp.sum(mix * mix, axis=1), 'kv')  21.7 us
    psum x1, blocking collectives, shards(): lax.psum((query_part, key_part, value_part, squares), 'kv')  20.1 us
    psum x1, waiting for transfers between devices, shards(): mix = lax.psum(mix_part, 'tp')  13.9 us
    dot_general x15, matrix products, extend(): return direct + jnp.einsum('sij,sjk->sik', direct, above)  13.1 us
    unnamed x42, local copies, waits for them, and re-layouts  7.95 us
    mul x8, local copies, waits for them, and re-layouts, head_norm(): return (grouped * factor * gain).reshape(raw.shape).astype(jnp.bfloat16)  5.91 us
  transfers between devices with their start and end apart: 3, of which 3 were waited for; matrix products, arithmetic and copies ran while one was open for 10% of the time, Pallas kernels for 0%

commit v1 on v0

v1 whole, which is shorter than its diff:
```python
import functools

import jax
import jax.numpy as jnp
from jax import lax
from jax.experimental import pallas as pl
from jax.experimental.pallas import tpu as pltpu
from jax.sharding import PartitionSpec as P

D = 4096
HEAD_DIM = 64
epsilon = 1e-05
MESH = pl.DeviceIdType.MESH
F32 = jnp.float32
BF16 = jnp.bfloat16


def iota(shape, axis):
    return lax.broadcasted_iota(jnp.int32, shape, axis)


def dot(a, b):
    return jnp.dot(a, b, preferred_element_type=F32)


def dot_t(a, b):
    return lax.dot_general(a, b, (((1,), (1,)), ((), ())), preferred_element_type=F32)


def exact_dot(a, ones):
    high = a.astype(BF16)
    rest = a - high.astype(F32)
    middle = rest.astype(BF16)
    low = (rest - middle.astype(F32)).astype(BF16)
    return dot(high, ones) + dot(middle, ones) + dot(low, ones)


def pack(rows):
    block = jnp.bitwise_and(iota((8, rows.shape[1]), 1), HEAD_DIM - 1) >> 3
    out = jnp.zeros((8, rows.shape[1]), F32)
    for j in range(rows.shape[0] // 8):
        out = jnp.where(block == j, rows[8 * j : 8 * j + 8], out)
    return out


def spread(packed, rows):
    inner = jnp.bitwise_and(iota(packed.shape, 1), HEAD_DIM - 1)
    return jnp.concatenate(
        [jnp.where(inner == 8 * j, packed, 0.0) for j in range(rows // 8)], axis=0
    )


def unpack_column(packed, rows):
    wide = spread(packed, rows)
    return jnp.sum(jnp.where(iota(wide.shape, 1) < HEAD_DIM, wide, 0.0), axis=1, keepdims=True)


def per_head(columns, width):
    lane_head = iota((columns[0].shape[0], width), 1) // HEAD_DIM
    out = jnp.broadcast_to(columns[0], lane_head.shape)
    for h in range(1, len(columns)):
        out = jnp.where(lane_head == h, columns[h], out)
    return out


def soft_stay(score):
    return -(jnp.maximum(score, 0.0) + jnp.log1p(jnp.exp(-jnp.abs(score))))


def greet(peers):
    barrier = pltpu.get_barrier_semaphore()
    for where in peers:
        pl.semaphore_signal(barrier, inc=1, device_id=where, device_id_type=MESH)
    pl.semaphore_wait(barrier, len(peers))


def head_norm(raw, gain):
    width = raw.shape[1]
    lane_head = iota(raw.shape, 1) // HEAD_DIM
    square = raw * raw
    means = [
        jnp.sum(jnp.where(lane_head == h, square, 0.0), axis=1, keepdims=True) / HEAD_DIM
        for h in range(width // HEAD_DIM)
    ]
    factor = per_head([lax.rsqrt(m + epsilon) for m in means], width)
    return (raw * factor * gain).astype(BF16)


def project_kernel(
    n,
    width,
    tokens_ref,
    norm_ref,
    wq_hbm,
    wk_hbm,
    wv_hbm,
    qgain_ref,
    kgain_ref,
    bias_ref,
    parents_ref,
    q_out,
    k_out,
    v_out,
    tree_sum_out,
    tree_exp_out,
    wq,
    wk,
    wv,
    send,
    recv,
    mine,
    gath,
    load_sem,
    send_sem,
    recv_sem,
    gsend_sem,
    grecv_sem,
):
    me = lax.axis_index("kv")
    loads = [
        pltpu.make_async_copy(a, b, load_sem.at[i])
        for i, (a, b) in enumerate(((wq_hbm, wq), (wk_hbm, wk), (wv_hbm, wv)))
    ]
    for load in loads:
        load.start()
    greet([{"kv": lax.rem(me + d, n)} for d in range(1, n)])
    rows = tokens_ref.shape[0]
    w = send.shape[2]
    wide = tokens_ref[...].astype(F32)
    scaled = (wide * norm_ref[...]).astype(BF16)
    squares = jnp.sum(wide * wide, axis=1, keepdims=True)
    squares = pack(jnp.broadcast_to(squares, (rows, w)))
    for load in loads:
        load.wait()

    def scatter(p):
        return pltpu.make_async_remote_copy(
            src_ref=send.at[p],
            dst_ref=recv.at[me],
            send_sem=send_sem.at[p],
            recv_sem=recv_sem.at[me],
            device_id={"kv": p},
            device_id_type=MESH,
        )

    total = n * w
    chunk = 256
    for c in range(0, total, chunk):
        for i, weight in enumerate((wq, wk, wv)):
            part = dot(scaled, weight[:, c : c + chunk])
            for p in range(c // w, (c + chunk) // w):
                send[p, i * rows : (i + 1) * rows, :] = part[:, p * w - c : (p + 1) * w - c]
        for p in range(c // w, (c + chunk) // w):
            send[p, 3 * rows :, :] = squares

            @pl.when(p != me)
            def _():
                scatter(p).start()

    owner = iota((rows, rows), 0) // width
    column = iota((rows, rows), 1)
    parents = parents_ref[...]
    direct = (column - owner * width == parents) & (column // width == owner)
    step = jnp.where(direct, 1.0, 0.0)
    reach = step
    span = 1
    while span < width:
        reach = reach + dot(reach.astype(BF16), step.astype(BF16))
        step = dot(step.astype(BF16), step.astype(BF16))
        span *= 2

    def from_peer(buffer, sem, ssem, source):
        return pltpu.make_async_remote_copy(
            src_ref=buffer.at[source],
            dst_ref=buffer.at[source],
            send_sem=ssem.at[source],
            recv_sem=sem.at[source],
            device_id={"kv": source},
            device_id_type=MESH,
        )

    summed = send[me]
    for d in range(1, n):
        source = lax.rem(me + d, n)
        from_peer(recv, recv_sem, send_sem, source).wait_recv()
        summed = summed + recv[source]
    query_raw = summed[:rows]
    key_raw = summed[rows : 2 * rows]
    value_raw = summed[2 * rows : 3 * rows]
    inv_rms = lax.rsqrt(unpack_column(summed[3 * rows :], rows) / D + epsilon)
    queries = head_norm(query_raw, qgain_ref[...])
    new_keys = head_norm(key_raw, kgain_ref[...])
    new_values = (value_raw * inv_rms).astype(BF16)
    mine[0:rows, :] = queries
    mine[rows : 2 * rows, :] = new_keys
    mine[2 * rows : 3 * rows, :] = new_values

    def spread_out(p):
        return pltpu.make_async_remote_copy(
            src_ref=mine,
            dst_ref=gath.at[me],
            send_sem=gsend_sem.at[p],
            recv_sem=grecv_sem.at[me],
            device_id={"kv": p},
            device_id_type=MESH,
        )

    for d in range(1, n):
        spread_out(lax.rem(me + d, n)).start()
    gath[me] = mine[...]

    heads = w // HEAD_DIM
    lane_head = iota((rows, w), 1) // HEAD_DIM
    sums, exps = [], []
    tri = jnp.where(iota((rows, rows), 0) > iota((rows, rows), 1), 1.0, 0.0).astype(BF16)
    mask = reach > 0.5
    for h in range(heads):
        only = jnp.where(lane_head == h, queries.astype(F32), 0.0).astype(BF16)
        score = dot_t(only, new_keys) * (HEAD_DIM ** (-0.5))
        score = score + bias_ref[0:1, h : h + 1]
        stay = soft_stay(score)
        taken = score + stay
        stay = jnp.where(mask, stay, 0.0)
        tail = exact_dot(stay, tri)
        weight = jnp.where(mask, jnp.exp(taken + tail), 0.0).astype(BF16)
        sums.append(dot(weight, new_values))
        exps.append(jnp.exp(jnp.sum(stay, axis=1, keepdims=True)))
    tree_sum = sums[0]
    for h in range(1, heads):
        tree_sum = jnp.where(lane_head == h, sums[h], tree_sum)
    tree_sum_out[...] = tree_sum
    tree_exp_out[...] = per_head(exps, w)

    for p in range(n):

        @pl.when(p != me)
        def _():
            from_peer(gath, grecv_sem, gsend_sem, p).wait_recv()

        q_out[:, p * w : (p + 1) * w] = gath[p, 0:rows, :]
        k_out[:, p * w : (p + 1) * w] = gath[p, rows : 2 * rows, :]
        v_out[:, p * w : (p + 1) * w] = gath[p, 2 * rows : 3 * rows, :]
    for d in range(1, n):
        peer = lax.rem(me + d, n)
        scatter(peer).wait_send()
        spread_out(peer).wait_send()


def cache_kernel(
    n,
    width,
    base_ref,
    accepted_ref,
    bias_ref,
    q_ref,
    k_ref,
    v_ref,
    ck_ref,
    cv_ref,
    pay_ref,
    uk_ref,
    uv_ref,
):
    me = lax.axis_index("kv")
    s = pl.program_id(0)
    span = ck_ref.shape[1]
    total = ck_ref.shape[2]
    w = pay_ref.shape[2]
    rows = pay_ref.shape[1] - 8
    valid = base_ref[s] + accepted_ref[s]
    start = me * span
    group = 256
    heads = group // HEAD_DIM
    own = iota((heads * width, group), 0) // width == iota((heads * width, group), 1) // HEAD_DIM
    scores = []
    for c in range(0, total, group):
        q = q_ref[:, c : c + group].astype(F32)
        diagonal = jnp.where(own, jnp.concatenate([q] * heads, axis=0), 0.0).astype(BF16)
        scores.append(dot_t(diagonal, ck_ref[0, :, c : c + group]))
    score = jnp.concatenate(scores, axis=0) * (HEAD_DIM ** (-0.5)) + bias_ref[...]
    live = start + iota(score.shape, 1) < valid
    stay = soft_stay(score)
    taken = score + stay
    stay = jnp.where(live, stay, 0.0)
    tri = jnp.where(iota((span, span), 0) > iota((span, span), 1), 1.0, 0.0).astype(BF16)
    tail = exact_dot(stay, tri)
    weight = jnp.where(live, jnp.exp(taken + tail), 0.0).astype(BF16)
    logs = jnp.sum(stay, axis=1, keepdims=True)
    at = pl.multiple_of(s * width, width)
    for g, c in enumerate(range(0, total, group)):
        r = slice(g * heads * width, (g + 1) * heads * width)
        full = jnp.where(own, dot(weight[r], cv_ref[0, :, c : c + group]), 0.0)
        log_full = jnp.where(own, logs[r], 0.0)
        block = full[0:width]
        log_block = log_full[0:width]
        for h in range(1, heads):
            block = block + full[h * width : (h + 1) * width]
            log_block = log_block + log_full[h * width : (h + 1) * width]
        for p in range(c // w, (c + group) // w):
            lanes = slice(p * w - c, (p + 1) * w - c)
            pay_ref[p, pl.ds(at, width), :] = block[:, lanes]
            slot = jnp.bitwise_and(iota((8, w), 1), HEAD_DIM - 1) >> 3
            packed = jnp.where(s == 0, jnp.zeros((8, w), F32), pay_ref[p, rows : rows + 8, :])
            for j in range(width // 8):
                packed = jnp.where(
                    slot == s * (width // 8) + j, log_block[8 * j : 8 * j + 8, lanes], packed
                )
            pay_ref[p, rows : rows + 8, :] = packed
    uk_ref[...] = ck_ref[...]
    uv_ref[...] = cv_ref[...]

    @pl.when((valid + width > start) & (valid < start + span))
    def _():
        offset = start + iota((span, width), 0) - valid
        chooser = jnp.where(offset == iota((span, width), 1), 1.0, 0.0).astype(BF16)
        offset = start + iota((span, total), 0) - valid
        inside = (offset >= 0) & (offset < width)
        for fresh, old, out in ((k_ref, ck_ref, uk_ref), (v_ref, cv_ref, uv_ref)):
            placed = dot(chooser, fresh[...])
            out[0] = jnp.where(inside, placed, old[0].astype(F32)).astype(BF16)


def output_kernel(
    n,
    pay_ref,
    tree_sum_ref,
    tree_exp_ref,
    wo_hbm,
    out_ref,
    wo,
    recv,
    att,
    gath,
    wide,
    part,
    other,
    sq,
    sqs,
    load_sem,
    send_sem,
    recv_sem,
    gsend_sem,
    grecv_sem,
    pair_sem,
    ssend_sem,
    srecv_sem,
):
    me = lax.axis_index("kv")
    core = lax.axis_index("tp")
    cores = lax.axis_size("tp")
    load = pltpu.make_async_copy(wo_hbm, wo, load_sem)
    load.start()
    peers = [lax.rem(me + d, n) for d in range(1, n)]
    partners = [lax.rem(core + d, cores) for d in range(1, cores)]
    greet([{"kv": p} for p in peers] + [{"tp": t} for t in partners])

    def push(src, dst, ssem, rsem, p):
        return pltpu.make_async_remote_copy(
            src_ref=src,
            dst_ref=dst.at[me],
            send_sem=ssem.at[p],
            recv_sem=rsem.at[me],
            device_id={"kv": p},
            device_id_type=MESH,
        )

    def arrived(dst, ssem, rsem, p):
        pltpu.make_async_remote_copy(
            src_ref=dst.at[p],
            dst_ref=dst.at[p],
            send_sem=ssem.at[p],
            recv_sem=rsem.at[p],
            device_id={"kv": p},
            device_id_type=MESH,
        ).wait_recv()

    for p in peers:
        push(pay_ref.at[p], recv, send_sem, recv_sem, p).start()
    recv[me] = pay_ref[me]
    rows, w = att.shape
    for p in peers:
        arrived(recv, send_sem, recv_sem, p)
    later = jnp.zeros((8, w), F32)
    scales = [None] * n
    for b in range(n - 1, -1, -1):
        scales[b] = spread(jnp.exp(later), rows)
        later = later + recv[b, rows : rows + 8, :]
    same = iota((w, w), 0) // HEAD_DIM == iota((w, w), 1) // HEAD_DIM
    same = jnp.where(same, 1.0, 0.0).astype(BF16)
    scale = exact_dot(jnp.concatenate(scales, axis=0), same)
    cache_part = jnp.zeros((rows, w), F32)
    for b in range(n):
        cache_part = cache_part + scale[b * rows : (b + 1) * rows] * recv[b, 0:rows, :]
    attended = tree_sum_ref[...] + tree_exp_ref[...] * cache_part
    att[...] = attended.astype(BF16)
    for p in peers:
        push(att, gath, gsend_sem, grecv_sem, p).start()
    gath[me] = att[...]
    load.wait()
    for p in range(n):

        @pl.when(p != me)
        def _():
            arrived(gath, gsend_sem, grecv_sem, p)

        wide[:, p * w : (p + 1) * w] = gath[p]
    part[...] = dot(wide[...], wo[...])
    swaps = [
        pltpu.make_async_remote_copy(
            src_ref=part,
            dst_ref=other.at[d],
            send_sem=pair_sem.at[0, d],
            recv_sem=pair_sem.at[1, d],
            device_id={"tp": t},
            device_id_type=MESH,
        )
        for d, t in enumerate(partners)
    ]
    for swap in swaps:
        swap.start()
    mix = part[...]
    for d, swap in enumerate(swaps):
        swap.wait_recv()
        mix = mix + other[d]
    squares = jnp.sum(mix * mix, axis=1, keepdims=True)
    sq[...] = pack(jnp.broadcast_to(squares, (rows, 128)))
    for p in peers:
        push(sq, sqs, ssend_sem, srecv_sem, p).start()
    sqs[me] = sq[...]
    for p in peers:
        arrived(sqs, ssend_sem, srecv_sem, p)
    total = sqs[0]
    for b in range(1, n):
        total = total + sqs[b]
    inv = lax.rsqrt(unpack_column(total, rows) / D + epsilon)
    out_ref[...] = (mix * inv).astype(BF16)
    for p in peers:
        push(pay_ref.at[p], recv, send_sem, recv_sem, p).wait_send()
        push(att, gath, gsend_sem, grecv_sem, p).wait_send()
        push(sq, sqs, ssend_sem, srecv_sem, p).wait_send()
    for swap in swaps:
        swap.wait_send()


def shards(
    n,
    tokens,
    norm_gain,
    w_query,
    w_key,
    w_value,
    query_gain,
    key_gain,
    head_bias,
    w_output,
    cache_keys,
    cache_values,
    base_length,
    accepted,
    parents,
):
    rows, depth = tokens.shape
    total = w_query.shape[1]
    w = total // n
    heads = w // HEAD_DIM
    seqs, width = parents.shape
    span = cache_keys.shape[1]
    columns = w_output.shape[1]
    vmem = pl.BlockSpec(memory_space=pltpu.VMEM)
    smem = pl.BlockSpec(memory_space=pltpu.SMEM)
    hbm = pl.BlockSpec(memory_space=pl.ANY)
    dma = pltpu.SemaphoreType.DMA
    mine_at = lax.axis_index("kv") * heads
    my_bias = lax.dynamic_slice(head_bias, (mine_at,), (heads,)).reshape(1, heads)
    queries, new_keys, new_values, tree_sum, tree_exp = pl.pallas_call(
        functools.partial(project_kernel, n, width),
        name="project",
        out_shape=[jax.ShapeDtypeStruct((rows, total), BF16)] * 3
        + [jax.ShapeDtypeStruct((rows, w), F32)] * 2,
        in_specs=[vmem, vmem, hbm, hbm, hbm, vmem, vmem, vmem, vmem],
        out_specs=[vmem] * 5,
        scratch_shapes=[
            pltpu.VMEM((depth, total), BF16),
            pltpu.VMEM((depth, total), BF16),
            pltpu.VMEM((depth, total), BF16),
            pltpu.VMEM((n, 3 * rows + 8, w), F32),
            pltpu.VMEM((n, 3 * rows + 8, w), F32),
            pltpu.VMEM((3 * rows, w), BF16),
            pltpu.VMEM((n, 3 * rows, w), BF16),
            dma((3,)),
            dma((n,)),
            dma((n,)),
            dma((n,)),
            dma((n,)),
        ],
        compiler_params=pltpu.CompilerParams(
            collective_id=0, has_side_effects=True, vmem_limit_bytes=32 * 2**20
        ),
    )(
        tokens,
        norm_gain.reshape(1, depth),
        w_query,
        w_key,
        w_value,
        jnp.tile(query_gain, heads).reshape(1, w),
        jnp.tile(key_gain, heads).reshape(1, w),
        my_bias,
        parents.reshape(rows, 1),
    )
    block = pl.BlockSpec((1, span, total), lambda s: (s, 0, 0))
    fresh = pl.BlockSpec((width, total), lambda s: (s, 0))
    pay, updated_keys, updated_values = pl.pallas_call(
        functools.partial(cache_kernel, n, width),
        name="cache",
        grid=(seqs,),
        out_shape=[
            jax.ShapeDtypeStruct((n, rows + 8, w), F32),
            jax.ShapeDtypeStruct(cache_keys.shape, BF16),
            jax.ShapeDtypeStruct(cache_values.shape, BF16),
        ],
        in_specs=[
            smem,
            smem,
            pl.BlockSpec((total // HEAD_DIM * width, 1), lambda s: (0, 0)),
            fresh,
            fresh,
            fresh,
            block,
            block,
        ],
        out_specs=[pl.BlockSpec((n, rows + 8, w), lambda s: (0, 0, 0)), block, block],
        compiler_params=pltpu.CompilerParams(
            dimension_semantics=("arbitrary",), vmem_limit_bytes=32 * 2**20
        ),
    )(
        base_length,
        accepted,
        jnp.repeat(head_bias, width).reshape(-1, 1),
        queries,
        new_keys,
        new_values,
        cache_keys,
        cache_values,
    )
    layer_out = pl.pallas_call(
        functools.partial(output_kernel, n),
        name="output",
        out_shape=jax.ShapeDtypeStruct((rows, columns), BF16),
        in_specs=[vmem, vmem, vmem, hbm],
        out_specs=vmem,
        scratch_shapes=[
            pltpu.VMEM(w_output.shape, BF16),
            pltpu.VMEM((n, rows + 8, w), F32),
            pltpu.VMEM((rows, w), BF16),
            pltpu.VMEM((n, rows, w), BF16),
            pltpu.VMEM((rows, total), BF16),
            pltpu.VMEM((rows, columns), F32),
            pltpu.VMEM((1, rows, columns), F32),
            pltpu.VMEM((8, 128), F32),
            pltpu.VMEM((n, 8, 128), F32),
            dma,
            dma((n,)),
            dma((n,)),
            dma((n,)),
            dma((n,)),
            dma((2, 1)),
            dma((n,)),
            dma((n,)),
        ],
        compiler_params=pltpu.CompilerParams(
            collective_id=1, has_side_effects=True, vmem_limit_bytes=32 * 2**20
        ),
    )(pay, tree_sum, tree_exp, w_output)
    return layer_out, updated_keys, updated_values


def solution(mesh):
    return jax.shard_map(
        functools.partial(shards, mesh.shape["kv"]),
        mesh=mesh,
        in_specs=(
            P("dp", "kv"),
            P("kv"),
            P("kv", "tp"),
            P("kv", "tp"),
            P("kv", "tp"),
            P(),
            P(),
            P("tp"),
            P("tp", "kv"),
            P("dp", "kv", "tp"),
            P("dp", "kv", "tp"),
            P("dp"),
            P("dp"),
            P("dp", None),
        ),
        out_specs=(P("dp", "kv"), P("dp", "kv", "tp"), P("dp", "kv", "tp")),
        check_vma=False,
    )
```

time: 291 us -> 75 us (0.26)
  waiting for transfers between devices: 120 us -> 0 us
  blocking collectives: 72.6 us -> 0 us
  Pallas kernels: 0 us -> 62.4 us
  matrix products: 35.5 us -> 0 us
  other arithmetic: 23.7 us -> 0 us
  between operations: 14 us -> 0.72 us
  local copies, waits for them, and re-layouts: 22.6 us -> 11.4 us
    psum x3 -> x0, waiting for transfers between devices: 120 us -> none  [the longest x2 106 us: shards(): lax.psum((query_part, key_part, value_part, squares), 'kv')]
    pallas_call x0 -> x3, Pallas kernels: none -> 62.4 us  [the longest x1 37 us: shards(): pl.pallas_call(functools.partial(project_kernel, n, width), name='project...]
    psum x2 -> x0, blocking collectives: 41.8 us -> none  [the longest x1 21.7 us: shards(): out_squares = lax.psum(jnp.sum(mix * mix, axis=1), 'kv')]
    dot_general x26 -> x0, matrix products: 35.5 us -> none  [the longest x15 13.1 us: extend(): return direct + jnp.einsum('sij,sjk->sik', direct, above)]
    all_gather x1 -> x0, blocking collectives: 30.9 us -> none  [carried_in(): pieces = lax.all_gather(value, axis)]
    mul x10 -> x0, local copies, waits for them, and re-layouts: 9.68 us -> none  [the longest x8 5.91 us: head_norm(): return (grouped * factor * gain).reshape(raw.shape).astype(jnp.bfloat16)]
    select_n x8 -> x0, other arithmetic: 7.63 us -> none  [the longest x7 5.35 us: step(): return jnp.where(position < mine, longer, running)]
    reduce_sum x6 -> x0, other arithmetic: 5.42 us -> none  [the longest x2 3.12 us: head_norm(): jnp.mean(grouped * grouped, axis=2, keepdims=True) + epsilon]
  transfers between devices with their start and end apart: 3 -> 0, of which waited for: 3 -> 0; matrix products, arithmetic and copies ran while one was open for 10% -> 0% of each run, Pallas kernels for 0% -> 0%
where the time goes in v1:
time: 75 us; the launch traced here: 74.4 us
  Pallas kernels  62.4 us (83%)
  local copies, waits for them, and re-layouts  11.4 us (15%)
    pallas_call x1, Pallas kernels, shards(): pl.pallas_call(functools.partial(project_kernel, n, width), name='project...  37 us
    pallas_call x1, Pallas kernels, shards(): pl.pallas_call(functools.partial(output_kernel, n), name='output', out_sh...  20.2 us
    unnamed x21, local copies, waits for them, and re-layouts  7.42 us
    pallas_call x1, Pallas kernels, shards(): pl.pallas_call(functools.partial(cache_kernel, n, width), name='cache', g...  5.14 us

profile of v1, /device:TPU:0, one launch (start us, length us, event | category | flops | bytes accessed | tf_op | source)
XLA Modules:
  0.0 74.4 jit_solution(1602703035092057093)
XLA Ops:
  0.6 0.0 copy-start
  0.6 0.9 %dynamic-slice_bitcast_fusion.bias_ref = f32[1,2]{1,0:T(1,128)S(1)} fusion(f32[16]{0:T(128)} %param.21, s32[]{:T(128)S(6)} %select_n.3), kind=kLoop, calls=%fused_computation | loop fusion | bytes 20 | tf_op jit(solution)/shard_map/reshape | solution.py:474
  1.5 0.7 tile.4
  2.2 0.1 reshape_tile.6.qgain_ref
  2.3 0.7 tile.5
  2.9 0.1 reshape_tile.7.kgain_ref
  3.0 0.7 broadcast_in_dim.3
  3.7 0.8 %reshape.20.parents_ref = s32[64,1]{1,0:T(8,128)S(1)} reshape(s32[4,16]{1,0:T(4,128)} %param.27) | data formatting | bytes 512 | tf_op jit(solution)/shard_map/reshape | solution.py:508
  4.5 0.1 reshape_reshape.4.bias_ref
  4.6 0.0 copy-start.2
  4.6 1.2 %copy-done.2 = bf16[512,1024]{1,0:T(8,128)(2,1)S(1)} copy-done((bf16[512,1024]{1,0:T(8,128)(2,1)S(1)}, bf16[512,1024]{1,0:T(8,128)(2,1)}, u32[]{:S(2)}) %copy-start.2) | copy-done | bytes 1048600
  5.8 0.0 copy-start.3
  5.8 1.2 %copy-done.3 = bf16[512,1024]{1,0:T(8,128)(2,1)S(1)} copy-done((bf16[512,1024]{1,0:T(8,128)(2,1)S(1)}, bf16[512,1024]{1,0:T(8,128)(2,1)}, u32[]{:S(2)}) %copy-start.3) | copy-done | bytes 1048600
  7.1 0.0 copy-start.4
  7.1 1.2 %copy-done.4 = bf16[512,1024]{1,0:T(8,128)(2,1)S(1)} copy-done((bf16[512,1024]{1,0:T(8,128)(2,1)S(1)}, bf16[512,1024]{1,0:T(8,128)(2,1)}, u32[]{:S(2)}) %copy-start.4) | copy-done | bytes 1048600
  8.3 0.0 copy-start.6
  8.3 0.8 %copy-done.6 = bf16[64,512]{1,0:T(8,128)(2,1)S(1)} copy-done((bf16[64,512]{1,0:T(8,128)(2,1)S(1)}, bf16[64,512]{1,0:T(8,128)(2,1)}, u32[]{:S(2)}) %copy-start.6) | copy-done | bytes 65560
  9.1 0.0 copy-start.7
  9.1 0.7 copy-done.7
  9.8 0.0 copy-start.8
  9.8 0.0 copy-start.9
  9.8 37.0 %project.1 = (bf16[64,1024]{1,0:T(8,128)(2,1)S(1)}, bf16[64,1024]{1,0:T(8,128)(2,1)S(1)}, bf16[64,1024]{1,0:T(8,128)(2,1)S(1)}, f32[64,128]{1,0:T(8,128)S(1)}, f32[64,128]{1,0:T(8,128)S(1)}) custom-call(bf16[64,512]{1,0:T(8,128)(2,1)S(1)} %copy-done.6, f32[1,512]{1,0:T(1,128)S(1)} %bitcast.3, bf16[512,1024]{1,0:T(8,128)(2,1)S(1)} %copy-done.2, ...), custom_call_target="tpu_custom_call" | custom-call | tf_op jit(solution)/shard_map/project/pallas_call | solution.py:475
  46.8 0.0 copy-done
  46.8 0.0 copy-done.8
  46.8 0.0 copy-done.9
  46.9 0.0 copy-start.1
  46.9 1.6 %copy-done.1 = bf16[4,256,1024]{2,1,0:T(8,128)(2,1)S(1)} copy-done((bf16[4,256,1024]{2,1,0:T(8,128)(2,1)S(1)}, bf16[4,256,1024]{2,1,0:T(8,128)(2,1)}, u32[]{:S(2)}) %copy-start.1) | copy-done | bytes 2097176
  48.5 0.0 copy-start.5
  48.5 5.1 %cache.1 = (f32[8,72,128]{2,1,0:T(8,128)S(1)}, bf16[4,256,1024]{2,1,0:T(8,128)(2,1)}, bf16[4,256,1024]{2,1,0:T(8,128)(2,1)}) custom-call(s32[4]{0:T(128)S(1)} %copy-done.8, s32[4]{0:T(128)S(1)} %copy-done.9, f32[256,1]{1,0:T(8,128)S(1)} %reshape_reshape.4.bias_ref, bf16[64,1024]{1,0:T(8,128)(2,1)S(1)} %get-tuple-element.11.q_ref, ...), custom_call_target="tpu_custom_call" | custom-call | tf_op jit(solution)/shard_map/cache/pallas_call | solution.py:512
  53.6 0.0 copy-done.5
  53.6 20.2 %output.1 = bf16[64,512]{1,0:T(8,128)(2,1)S(1)} custom-call(f32[8,72,128]{2,1,0:T(8,128)S(1)} %get-tuple-element.14.pay_ref, f32[64,128]{1,0:T(8,128)S(1)} %get-tuple-element.15.tree_sum_ref, f32[64,128]{1,0:T(8,128)S(1)} %get-tuple-element.16.tree_exp_ref, bf16[1024,512]{1,0:T(8,128)(2,1)S(1)} %copy-done.5), custom_call_target="tpu_custom_call" | custom-call | tf_op jit(solution)/shard_map/output/pallas_call | solution.py:545
  73.8 0.6 copy.21
Async XLA Ops:
  0.6 46.2 %copy-start = (bf16[4,256,1024]{2,1,0:T(8,128)(2,1)S(1)}, bf16[4,256,1024]{2,1,0:T(8,128)(2,1)}, u32[]{:S(2)}) copy-start(bf16[4,256,1024]{2,1,0:T(8,128)(2,1)} %ck_ref.1) | copy-start | bytes 6291460
  4.6 1.2 %copy-start.2 = (bf16[512,1024]{1,0:T(8,128)(2,1)S(1)}, bf16[512,1024]{1,0:T(8,128)(2,1)}, u32[]{:S(2)}) copy-start(bf16[512,1024]{1,0:T(8,128)(2,1)} %wq_hbm.1) | copy-start | bytes 3145732
  5.8 1.2 %copy-start.3 = (bf16[512,1024]{1,0:T(8,128)(2,1)S(1)}, bf16[512,1024]{1,0:T(8,128)(2,1)}, u32[]{:S(2)}) copy-start(bf16[512,1024]{1,0:T(8,128)(2,1)} %wk_hbm.1) | copy-start | bytes 3145732
  7.1 1.2 %copy-start.4 = (bf16[512,1024]{1,0:T(8,128)(2,1)S(1)}, bf16[512,1024]{1,0:T(8,128)(2,1)}, u32[]{:S(2)}) copy-start(bf16[512,1024]{1,0:T(8,128)(2,1)} %wv_hbm.1) | copy-start | bytes 3145732
  8.3 0.8 %copy-start.6 = (bf16[64,512]{1,0:T(8,128)(2,1)S(1)}, bf16[64,512]{1,0:T(8,128)(2,1)}, u32[]{:S(2)}) copy-start(bf16[64,512]{1,0:T(8,128)(2,1)} %tokens_ref.1) | copy-start | bytes 196612
  9.1 0.7 copy-start.7
  9.8 37.0 %copy-start.8 = (s32[4]{0:T(128)S(1)}, s32[4]{0:T(128)}, u32[]{:S(2)}) copy-start(s32[4]{0:T(128)} %base_ref.1) | copy-start | bytes 52
  9.8 37.0 %copy-start.9 = (s32[4]{0:T(128)S(1)}, s32[4]{0:T(128)}, u32[]{:S(2)}) copy-start(s32[4]{0:T(128)} %accepted_ref.1) | copy-start | bytes 52
  46.9 1.6 %copy-start.1 = (bf16[4,256,1024]{2,1,0:T(8,128)(2,1)S(1)}, bf16[4,256,1024]{2,1,0:T(8,128)(2,1)}, u32[]{:S(2)}) copy-start(bf16[4,256,1024]{2,1,0:T(8,128)(2,1)} %cv_ref.1) | copy-start | bytes 6291460
  48.5 5.1 %copy-start.5 = (bf16[1024,512]{1,0:T(8,128)(2,1)S(1)}, bf16[1024,512]{1,0:T(8,128)(2,1)}, u32[]{:S(2)}) copy-start(bf16[1024,512]{1,0:T(8,128)(2,1)} %wo_hbm.1) | copy-start | bytes 3145732

commit v2 on v1

--- a/solution.py
+++ b/solution.py
@@ -107,16 +107,22 @@
     wk,
     wv,
     send,
+    half,
+    pairs,
     recv,
     mine,
     gath,
     load_sem,
+    hsend_sem,
+    hrecv_sem,
     send_sem,
     recv_sem,
     gsend_sem,
     grecv_sem,
 ):
     me = lax.axis_index("kv")
+    side = lax.rem(me, 2)
+    spot = me // 2
     loads = [
         pltpu.make_async_copy(a, b, load_sem.at[i])
         for i, (a, b) in enumerate(((wq_hbm, wq), (wk_hbm, wk), (wv_hbm, wv)))
@@ -133,13 +139,23 @@
     for load in loads:
         load.wait()
 
-    def scatter(p):
+    def to_pair(g):
         return pltpu.make_async_remote_copy(
-            src_ref=send.at[p],
-            dst_ref=recv.at[me],
-            send_sem=send_sem.at[p],
-            recv_sem=recv_sem.at[me],
-            device_id={"kv": p},
+            src_ref=send.at[2 * g + 1 - side],
+            dst_ref=half.at[g],
+            send_sem=hsend_sem.at[g],
+            recv_sem=hrecv_sem.at[g],
+            device_id={"kv": me + 1 - 2 * side},
+            device_id_type=MESH,
+        )
+
+    def scatter(g):
+        return pltpu.make_async_remote_copy(
+            src_ref=pairs.at[g],
+            dst_ref=recv.at[spot],
+            send_sem=send_sem.at[g],
+            recv_sem=recv_sem.at[spot],
+            device_id={"kv": 2 * g + side},
             device_id_type=MESH,
         )
 
@@ -152,10 +168,15 @@
                 send[p, i * rows : (i + 1) * rows, :] = part[:, p * w - c : (p + 1) * w - c]
         for p in range(c // w, (c + chunk) // w):
             send[p, 3 * rows :, :] = squares
-
-            @pl.when(p != me)
-            def _():
-                scatter(p).start()
+        for g in range(c // w // 2, (c + chunk) // w // 2):
+            to_pair(g).start()
+    for g in range(n // 2):
+        to_pair(g).wait_recv()
+        pairs[g] = send[2 * g + side] + half[g]
+
+        @pl.when(g != spot)
+        def _():
+            scatter(g).start()
 
     owner = iota((rows, rows), 0) // width
     column = iota((rows, rows), 1)
@@ -179,10 +200,17 @@
             device_id_type=MESH,
         )
 
-    summed = send[me]
-    for d in range(1, n):
-        source = lax.rem(me + d, n)
-        from_peer(recv, recv_sem, send_sem, source).wait_recv()
+    summed = pairs[spot]
+    for d in range(1, n // 2):
+        source = lax.rem(spot + d, n // 2)
+        pltpu.make_async_remote_copy(
+            src_ref=pairs.at[source],
+            dst_ref=recv.at[source],
+            send_sem=send_sem.at[source],
+            recv_sem=recv_sem.at[source],
+            device_id={"kv": 2 * source + side},
+            device_id_type=MESH,
+        ).wait_recv()
         summed = summed + recv[source]
     query_raw = summed[:rows]
     key_raw = summed[rows : 2 * rows]
@@ -242,8 +270,11 @@
         v_out[:, p * w : (p + 1) * w] = gath[p, 2 * rows : 3 * rows, :]
     for d in range(1, n):
         peer = lax.rem(me + d, n)
-        scatter(peer).wait_send()
         spread_out(peer).wait_send()
+    for d in range(1, n // 2):
+        scatter(lax.rem(spot + d, n // 2)).wait_send()
+    for g in range(n // 2):
+        to_pair(g).wait_send()
 
 
 def cache_kernel(
@@ -484,17 +515,21 @@
             pltpu.VMEM((depth, total), BF16),
             pltpu.VMEM((depth, total), BF16),
             pltpu.VMEM((n, 3 * rows + 8, w), F32),
-            pltpu.VMEM((n, 3 * rows + 8, w), F32),
+            pltpu.VMEM((n // 2, 3 * rows + 8, w), F32),
+            pltpu.VMEM((n // 2, 3 * rows + 8, w), F32),
+            pltpu.VMEM((n // 2, 3 * rows + 8, w), F32),
             pltpu.VMEM((3 * rows, w), BF16),
             pltpu.VMEM((n, 3 * rows, w), BF16),
             dma((3,)),
-            dma((n,)),
-            dma((n,)),
+            dma((n // 2,)),
+            dma((n // 2,)),
+            dma((n // 2,)),
+            dma((n // 2,)),
             dma((n,)),
             dma((n,)),
         ],
         compiler_params=pltpu.CompilerParams(
-            collective_id=0, has_side_effects=True, vmem_limit_bytes=32 * 2**20
+            collective_id=0, has_side_effects=True, vmem_limit_bytes=62 * 2**20
         ),
     )(
         tokens,

time: 75 us -> 76.1 us (1.015)
  local copies, waits for them, and re-layouts: 11.4 us -> 12.5 us
    unnamed x21, local copies, waits for them, and re-layouts: 7.42 us -> 6.54 us
where the time goes in v2:
time: 76.1 us; the launch traced here: 75.7 us
  Pallas kernels  62.5 us (82%)
  local copies, waits for them, and re-layouts  12.5 us (16%)
    pallas_call x1, Pallas kernels, shards(): pl.pallas_call(functools.partial(project_kernel, n, width), name='project...  36.6 us
    pallas_call x1, Pallas kernels, shards(): pl.pallas_call(functools.partial(output_kernel, n), name='output', out_sh...  20.8 us
    unnamed x21, local copies, waits for them, and re-layouts  6.54 us
    pallas_call x1, Pallas kernels, shards(): pl.pallas_call(functools.partial(cache_kernel, n, width), name='cache', g...  5.17 us

profile of v2, /device:TPU:0, one launch (start us, length us, event | category | flops | bytes accessed | tf_op | source)
XLA Modules:
  0.0 75.7 jit_solution(3036071830230574095)
XLA Ops:
  0.6 0.0 copy-start.9
  0.6 0.0 copy-start.8
  0.7 1.3 %dynamic-slice_bitcast_fusion.bias_ref = f32[1,2]{1,0:T(1,128)} fusion(f32[16]{0:T(128)} %param.21, s32[]{:T(128)S(6)} %select_n.3), kind=kLoop, calls=%fused_computation | loop fusion | bytes 20 | tf_op jit(solution)/shard_map/reshape | solution.py:505
  1.9 0.7 tile.4
  2.6 0.6 reshape_tile.6.qgain_ref
  3.2 0.7 tile.5
  3.8 0.6 reshape_tile.7.kgain_ref
  4.4 0.7 broadcast_in_dim.3
  5.1 1.4 %reshape.20.parents_ref = s32[64,1]{1,0:T(8,128)} reshape(s32[4,16]{1,0:T(4,128)} %param.27) | data formatting | bytes 512 | tf_op jit(solution)/shard_map/reshape | solution.py:543
  6.5 0.1 reshape_reshape.4.bias_ref
  6.6 36.6 %project.1 = (bf16[64,1024]{1,0:T(8,128)(2,1)}, bf16[64,1024]{1,0:T(8,128)(2,1)}, bf16[64,1024]{1,0:T(8,128)(2,1)}, f32[64,128]{1,0:T(8,128)}, f32[64,128]{1,0:T(8,128)}) custom-call(bf16[64,512]{1,0:T(8,128)(2,1)} %tokens_ref.1, f32[1,512]{1,0:T(1,128)} %bitcast.3, bf16[512,1024]{1,0:T(8,128)(2,1)} %wq_hbm.1, bf16[512,1024]{1,0:T(8,128)(2,1)} %wk_hbm.1, ...), custom_call_target="tpu_custom_call" | custom-call | tf_op jit(solution)/shard_map/project/pallas_call | solution.py:506
  43.2 0.0 copy-done.9
  43.2 0.0 copy-done.8
  43.2 0.0 copy-start
  43.2 1.6 %copy-done = bf16[4,256,1024]{2,1,0:T(8,128)(2,1)S(1)} copy-done((bf16[4,256,1024]{2,1,0:T(8,128)(2,1)S(1)}, bf16[4,256,1024]{2,1,0:T(8,128)(2,1)}, u32[]{:S(2)}) %copy-start) | copy-done | bytes 2097176
  44.8 0.0 copy-start.1
  44.8 1.6 %copy-done.1 = bf16[4,256,1024]{2,1,0:T(8,128)(2,1)S(1)} copy-done((bf16[4,256,1024]{2,1,0:T(8,128)(2,1)S(1)}, bf16[4,256,1024]{2,1,0:T(8,128)(2,1)}, u32[]{:S(2)}) %copy-start.1) | copy-done | bytes 2097176
  46.4 0.0 copy-start.3
  46.4 0.9 %copy-done.3 = bf16[64,1024]{1,0:T(8,128)(2,1)S(1)} copy-done((bf16[64,1024]{1,0:T(8,128)(2,1)S(1)}, bf16[64,1024]{1,0:T(8,128)(2,1)}, u32[]{:S(2)}) %copy-start.3) | copy-done | bytes 131096
  47.3 0.0 copy-start.4
  47.3 0.9 %copy-done.4 = bf16[64,1024]{1,0:T(8,128)(2,1)S(1)} copy-done((bf16[64,1024]{1,0:T(8,128)(2,1)S(1)}, bf16[64,1024]{1,0:T(8,128)(2,1)}, u32[]{:S(2)}) %copy-start.4) | copy-done | bytes 131096
  48.2 0.0 copy-start.5
  48.2 0.9 %copy-done.5 = bf16[64,1024]{1,0:T(8,128)(2,1)S(1)} copy-done((bf16[64,1024]{1,0:T(8,128)(2,1)S(1)}, bf16[64,1024]{1,0:T(8,128)(2,1)}, u32[]{:S(2)}) %copy-start.5) | copy-done | bytes 131096
  49.1 0.0 copy-start.2
  49.1 0.0 copy-start.6
  49.1 0.0 copy-start.7
  49.1 5.2 %cache.1 = (f32[8,72,128]{2,1,0:T(8,128)S(1)}, bf16[4,256,1024]{2,1,0:T(8,128)(2,1)}, bf16[4,256,1024]{2,1,0:T(8,128)(2,1)}) custom-call(s32[4]{0:T(128)S(1)} %copy-done.8, s32[4]{0:T(128)S(1)} %copy-done.9, f32[256,1]{1,0:T(8,128)S(1)} %reshape_reshape.4.bias_ref, bf16[64,1024]{1,0:T(8,128)(2,1)S(1)} %copy-done.3, bf16[64,1024]{1,0:T(8,128)(2,1)S(1)} %copy-done.4, ...), custom_call_target="tpu_custom_call" | custom-call | tf_op jit(solution)/shard_map/cache/pallas_call | solution.py:547
  54.3 0.0 copy-done.2
  54.3 0.0 copy-done.6
  54.3 0.0 copy-done.7
  54.3 20.8 %output.1 = bf16[64,512]{1,0:T(8,128)(2,1)S(1)} custom-call(f32[8,72,128]{2,1,0:T(8,128)S(1)} %get-tuple-element.14.pay_ref, f32[64,128]{1,0:T(8,128)S(1)} %copy-done.6, f32[64,128]{1,0:T(8,128)S(1)} %copy-done.7, bf16[1024,512]{1,0:T(8,128)(2,1)S(1)} %copy-done.2), custom_call_target="tpu_custom_call" | custom-call | tf_op jit(solution)/shard_map/output/pallas_call | solution.py:580
  75.1 0.6 copy.21
Async XLA Ops:
  0.6 42.6 %copy-start.9 = (s32[4]{0:T(128)S(1)}, s32[4]{0:T(128)}, u32[]{:S(2)}) copy-start(s32[4]{0:T(128)} %accepted_ref.1) | copy-start | bytes 52
  0.6 42.6 %copy-start.8 = (s32[4]{0:T(128)S(1)}, s32[4]{0:T(128)}, u32[]{:S(2)}) copy-start(s32[4]{0:T(128)} %base_ref.1) | copy-start | bytes 52
  43.2 1.6 %copy-start = (bf16[4,256,1024]{2,1,0:T(8,128)(2,1)S(1)}, bf16[4,256,1024]{2,1,0:T(8,128)(2,1)}, u32[]{:S(2)}) copy-start(bf16[4,256,1024]{2,1,0:T(8,128)(2,1)} %ck_ref.1) | copy-start | bytes 6291460
  44.8 1.6 %copy-start.1 = (bf16[4,256,1024]{2,1,0:T(8,128)(2,1)S(1)}, bf16[4,256,1024]{2,1,0:T(8,128)(2,1)}, u32[]{:S(2)}) copy-start(bf16[4,256,1024]{2,1,0:T(8,128)(2,1)} %cv_ref.1) | copy-start | bytes 6291460
  46.4 0.9 %copy-start.3 = (bf16[64,1024]{1,0:T(8,128)(2,1)S(1)}, bf16[64,1024]{1,0:T(8,128)(2,1)}, u32[]{:S(2)}) copy-start(bf16[64,1024]{1,0:T(8,128)(2,1)} %get-tuple-element.11.q_ref) | copy-start | bytes 393220
  47.3 0.9 %copy-start.4 = (bf16[64,1024]{1,0:T(8,128)(2,1)S(1)}, bf16[64,1024]{1,0:T(8,128)(2,1)}, u32[]{:S(2)}) copy-start(bf16[64,1024]{1,0:T(8,128)(2,1)} %get-tuple-element.12.k_ref) | copy-start | bytes 393220
  48.2 0.9 %copy-start.5 = (bf16[64,1024]{1,0:T(8,128)(2,1)S(1)}, bf16[64,1024]{1,0:T(8,128)(2,1)}, u32[]{:S(2)}) copy-start(bf16[64,1024]{1,0:T(8,128)(2,1)} %get-tuple-element.13.v_ref) | copy-start | bytes 393220
  49.1 5.2 %copy-start.2 = (bf16[1024,512]{1,0:T(8,128)(2,1)S(1)}, bf16[1024,512]{1,0:T(8,128)(2,1)}, u32[]{:S(2)}) copy-start(bf16[1024,512]{1,0:T(8,128)(2,1)} %wo_hbm.1) | copy-start | bytes 3145732
  49.1 5.2 %copy-start.6 = (f32[64,128]{1,0:T(8,128)S(1)}, f32[64,128]{1,0:T(8,128)}, u32[]{:S(2)}) copy-start(f32[64,128]{1,0:T(8,128)} %get-tuple-element.15.tree_sum_ref) | copy-start | bytes 98308
  49.1 5.2 %copy-start.7 = (f32[64,128]{1,0:T(8,128)S(1)}, f32[64,128]{1,0:T(8,128)}, u32[]{:S(2)}) copy-start(f32[64,128]{1,0:T(8,128)} %get-tuple-element.16.tree_exp_ref) | copy-start | bytes 98308
